TPU v7x, 32 devices: a whole 2x2x4 slice. The times are simulated.
32 devices in a mesh: kv: 8 (over z, y), tp: 4 (over x, core).
Axes of the slice: x: 2, y: 2, z: 4, core: 2. Of those that a mesh axis runs over, the one named last changes fastest.
Arguments:
- tokens: bfloat16 [32, 4096], P(None, 'kv'), may hold values from -8 to 8, as said below
- attn_gain: float32 [4096], P('kv'), may hold values from 0.1 to 1.9
- query_weight: bfloat16 [4096, 1024], P('kv', 'tp'), may hold values from -0.09375 to 0.09375
- key_weight: bfloat16 [4096, 1024], P('kv', 'tp'), may hold values from -0.09375 to 0.09375
- value_weight: bfloat16 [4096, 2048], P('kv', 'tp'), may hold values from -0.09375 to 0.09375
- outgate_weight: bfloat16 [4096, 2048], P('kv', 'tp'), may hold values from -0.09375 to 0.09375
- code_weight: bfloat16 [4096, 16], P('kv'), may hold values from -0.09375 to 0.09375
- decay_weight: bfloat16 [16, 1024], P(None, 'tp'), may hold values from -6 to 6
- decay_bias: float32 [1024], P('tp'), may hold values from -4 to 2
- head_gain: float32 [256], replicated, may hold values from 0.1 to 1.9
- key_cache: bfloat16 [32, 64, 8, 128], P('kv', None, 'tp'), may hold values from -6 to 6
- value_cache: bfloat16 [32, 64, 8, 256], P('kv', None, 'tp'), may hold values from -6 to 6
- decay_cache: float32 [32, 64, 8, 128], P('kv', None, 'tp'), may hold values from -1.1 to 0
- carried_state: float32 [32, 8, 128, 256], P('kv', 'tp'), may hold values from -24 to 24
- lengths: int32 [32], P('kv'), may hold values from 1 to 64, 832 in all
- output_weight: bfloat16 [2048, 4096], P('tp', 'kv'), may hold values from -0.125 to 0.125
- mlp_gain: float32 [4096], P('kv'), may hold values from 0.1 to 1.9
- gate_weight: bfloat16 [4096, 11008], P('kv', 'tp'), may hold values from -0.09375 to 0.09375
- up_weight: bfloat16 [4096, 11008], P('kv', 'tp'), may hold values from -0.09375 to 0.09375
- down_weight: bfloat16 [11008, 4096], P('tp', 'kv'), may hold values from -0.0546875 to 0.0546875
Outputs:
- layer_out: bfloat16 [32, 4096], P(None, 'kv')
- new_keys: bfloat16 [32, 8, 128], P('kv', 'tp')
- new_values: bfloat16 [32, 8, 256], P('kv', 'tp')
Inputs may be any that keep to these rules, and one draw needn't show every extreme that they name: `tokens`: the features of a row have unlike scales. Sequence b's new token comes right after its lengths[b] live positions; positions from lengths[b] on take no part.
All inputs are finite; a program needn't handle non-finite values. No bound on the sum of `lengths` on one device may be relied on, other than what follows from the above.
Results may differ from a plain program's by a relative error of at most 0.025.
Values may be sent and summed in bfloat16 or wider, within the bound.
A program may use at most 64 MiB of HBM per device.

v0:
```python
import jax
import jax.numpy as jnp
from jax import lax
from jax.sharding import PartitionSpec as P

WIDTH = 4096


EPS = 1e-06
GATE_TEMP = 16.0


def across_heads(partial_value):
    return lax.psum(partial_value.astype(jnp.bfloat16), "tp").astype(jnp.float32)


def block_attention(
    queries,
    new_keys,
    new_values,
    new_decay,
    key_cache,
    value_cache,
    decay_cache,
    carried_state,
    lengths,
):
    positions = jnp.arange(key_cache.shape[1], dtype=jnp.int32)
    live_mask = positions[None, :] < lengths[:, None]
    kept_decay = jnp.where(live_mask[:, :, None, None], decay_cache, jnp.zeros_like(decay_cache))
    later_sum = lax.cumsum(kept_decay, axis=1, reverse=True) - kept_decay
    total_decay = jnp.sum(kept_decay, axis=1)
    decayed = queries.astype(jnp.float32) * jnp.exp(new_decay)
    carried = jnp.einsum(
        "bhd,bhde->bhe",
        decayed * jnp.exp(total_decay),
        carried_state,
        precision=lax.Precision.HIGHEST,
    )
    keyed_cache = key_cache.astype(jnp.float32) * jnp.exp(later_sum)
    scores = jnp.einsum("bhd,bshd->bhs", decayed, keyed_cache, precision=lax.Precision.HIGHEST)
    scores = jnp.where(live_mask[:, None, :], scores, jnp.zeros_like(scores)).astype(jnp.bfloat16)
    within = jnp.einsum("bhs,bshe->bhe", scores, value_cache, preferred_element_type=jnp.float32)
    own_score = jnp.sum(queries.astype(jnp.float32) * new_keys.astype(jnp.float32), axis=-1)
    return carried + within + own_score[..., None] * new_values.astype(jnp.float32)


def mixer_hidden(gate_sum, up_sum, square_sum):
    inv_mid = lax.rsqrt(square_sum / WIDTH + EPS)[:, None]
    return (jax.nn.silu(gate_sum * inv_mid) * (up_sum * inv_mid)).astype(jnp.bfloat16)


def on_device(
    tokens,
    attn_gain,
    query_weight,
    key_weight,
    value_weight,
    outgate_weight,
    code_weight,
    decay_weight,
    decay_bias,
    head_gain,
    key_cache,
    value_cache,
    decay_cache,
    carried_state,
    lengths,
    output_weight,
    mlp_gain,
    gate_weight,
    up_weight,
    down_weight,
):
    local_seqs, heads_here, key_dim, value_dim = carried_state.shape
    token_f = tokens.astype(jnp.float32)
    scaled = (token_f * attn_gain[None, :]).astype(jnp.bfloat16)
    query_part = jnp.dot(scaled, query_weight, preferred_element_type=jnp.float32)
    key_part = jnp.dot(scaled, key_weight, preferred_element_type=jnp.float32)
    value_part = jnp.dot(scaled, value_weight, preferred_element_type=jnp.float32)
    outgate_part = jnp.dot(scaled, outgate_weight, preferred_element_type=jnp.float32)
    code_part = jnp.dot(scaled, code_weight, preferred_element_type=jnp.float32)
    token_squares = jnp.sum(token_f * token_f, axis=1)
    query_sum, key_sum, value_sum, outgate_sum, code_sum, square_sum = (
        lax.psum_scatter(
            query_part.astype(jnp.bfloat16), "kv", scatter_dimension=0, tiled=True
        ).astype(jnp.float32),
        lax.psum_scatter(
            key_part.astype(jnp.bfloat16), "kv", scatter_dimension=0, tiled=True
        ).astype(jnp.float32),
        lax.psum_scatter(
            value_part.astype(jnp.bfloat16), "kv", scatter_dimension=0, tiled=True
        ).astype(jnp.float32),
        lax.psum_scatter(
            outgate_part.astype(jnp.bfloat16), "kv", scatter_dimension=0, tiled=True
        ).astype(jnp.float32),
        lax.psum_scatter(
            code_part.astype(jnp.bfloat16), "kv", scatter_dimension=0, tiled=True
        ).astype(jnp.float32),
        lax.psum_scatter(
            token_squares.astype(jnp.bfloat16), "kv", scatter_dimension=0, tiled=True
        ).astype(jnp.float32),
    )
    inv_rms = lax.rsqrt(square_sum / WIDTH + EPS)[:, None]
    queries = (
        (query_sum * inv_rms * key_dim ** (-0.5))
        .astype(jnp.bfloat16)
        .reshape(local_seqs, heads_here, key_dim)
    )
    new_keys = (key_sum * inv_rms).astype(jnp.bfloat16).reshape(local_seqs, heads_here, key_dim)
    new_values = (
        (value_sum * inv_rms).astype(jnp.bfloat16).reshape(local_seqs, heads_here, value_dim)
    )
    out_gate = (
        (outgate_sum * inv_rms).astype(jnp.bfloat16).reshape(local_seqs, heads_here, value_dim)
    )
    gate_code = (code_sum * inv_rms).astype(jnp.bfloat16)
    pre_gate = (
        jnp.dot(gate_code, decay_weight, preferred_element_type=jnp.float32) + decay_bias[None, :]
    )
    new_decay = (jax.nn.log_sigmoid(pre_gate) / GATE_TEMP).reshape(local_seqs, heads_here, key_dim)
    mixed_heads = block_attention(
        queries,
        new_keys,
        new_values,
        new_decay,
        key_cache,
        value_cache,
        decay_cache,
        carried_state,
        lengths,
    )
    normed = (
        mixed_heads
        * lax.rsqrt(jnp.mean(mixed_heads * mixed_heads, axis=-1, keepdims=True) + EPS)
        * head_gain
    )
    heads_out = (
        (normed * jax.nn.silu(out_gate.astype(jnp.float32)))
        .astype(jnp.bfloat16)
        .reshape(local_seqs, heads_here * value_dim)
    )
    attended = across_heads(
        jnp.dot(
            lax.all_gather(heads_out, "kv", axis=0, tiled=True),
            output_weight,
            preferred_element_type=jnp.float32,
        )
    )
    middle = (token_f + attended).astype(jnp.bfloat16)
    mid_f = middle.astype(jnp.float32)
    scaled_mid = (mid_f * mlp_gain[None, :]).astype(jnp.bfloat16)
    gate_part = jnp.dot(scaled_mid, gate_weight, preferred_element_type=jnp.float32)
    up_part = jnp.dot(scaled_mid, up_weight, preferred_element_type=jnp.float32)
    mid_squares = jnp.sum(mid_f * mid_f, axis=1)
    gate_sum, up_sum, mid_sum = (
        lax.psum(gate_part.astype(jnp.bfloat16), "kv").astype(jnp.float32),
        lax.psum(up_part.astype(jnp.bfloat16), "kv").astype(jnp.float32),
        lax.psum(mid_squares.astype(jnp.bfloat16), "kv").astype(jnp.float32),
    )
    hidden = mixer_hidden(gate_sum, up_sum, mid_sum)
    lifted_part = jnp.dot(hidden, down_weight, preferred_element_type=jnp.float32)
    layer_out = (mid_f + across_heads(lifted_part)).astype(jnp.bfloat16)
    return (layer_out, new_keys, new_values)


def solution(mesh):
    in_specs = (
        P(None, "kv"),
        P("kv"),
        P("kv", "tp"),
        P("kv", "tp"),
        P("kv", "tp"),
        P("kv", "tp"),
        P("kv", None),
        P(None, "tp"),
        P("tp"),
        P(),
        P("kv", None, "tp", None),
        P("kv", None, "tp", None),
        P("kv", None, "tp", None),
        P("kv", "tp", None, None),
        P("kv"),
        P("tp", "kv"),
        P("kv"),
        P("kv", "tp"),
        P("kv", "tp"),
        P("tp", "kv"),
    )
    out_specs = (P(None, "kv"), P("kv", "tp", None), P("kv", "tp", None))
    return jax.shard_map(
        on_device, mesh=mesh, in_specs=in_specs, out_specs=out_specs, check_vma=False
    )
```

profile of v0, /device:TPU:0, one launch (start us, length us, event | category | flops | bytes accessed | tf_op | source)
XLA Modules:
  0.0 236.8 jit_solution(11415016828430029316)
XLA Ops:
  7.2 0.0 copy-start
  7.2 0.0 copy-start.2
  7.2 0.0 copy-start.9
  7.2 0.0 copy-start.8
  7.2 0.0 copy-start.7
  7.2 0.0 all-reduce.11.cloned.1.call-start
  7.3 1.5 fusion.11
  8.8 1.5 convolution_convert_fusion.8
  10.3 1.7 convolution_convert_fusion.7
  12.1 1.7 convolution_convert_fusion.6
  13.8 1.9 convolution_convert_fusion.5
  15.7 1.9 convolution_convert_fusion.4
  17.6 0.0 all-reduce.11.cloned.1.call-update
  17.6 0.0 all-reduce.13.cloned.1.call-start
  17.6 0.7 iota_compare_fusion
  18.4 1.2 dynamic-slice
  20.3 2.6 %exponential_multiply_fusion = f32[4,64,2,128]{3,2,1,0:T(2,128)S(1)} fusion(bf16[4,64,2,128]{3,2,1,0:T(2,128)(2,1)} %param.30, f32[4,64,2,128]{3,2,1,0:T(2,128)} %param.32, pred[4,64]{1,0:T(4,128)(4,1)S(1)} %iota_compare_fusion), kind=kOutput, calls=%fused_computation.16 | output fusion | flops 4456448 | bytes 655616 | tf_op jit(solution)/shard_map/block_attention/reduce_window_sum | solution.py:31
  22.9 0.0 copy-done.2
  22.9 0.3 fusion.8
  23.2 68.5 %all-reduce.11.cloned.1.call-done = (bf16[32,512]{1,0:T(8,128)(2,1)}, bf16[32]{0:T(256)(128)(2,1)}, bf16[32,256]{1,0:T(8,128)(2,1)}, bf16[32,16]{1,0:T(8,128)(2,...) async-done(((bf16[32,512]{1,0:T(8,128)(2,1)}, bf16[32]{0:T(256)(128)(2,1)}, bf16[32,256]{1,0:T(8,128)(2,1)}, bf16[32,16]{1,0:T(8,128)(2,1)}, ...) | async-done | bytes 99408
  91.8 0.7 fusion.36
  92.5 0.0 copy-done.9
  92.5 0.0 copy-done.8
  92.5 0.9 fusion.29
  93.4 0.8 multiply_convert_fusion.4
  94.2 0.8 multiply_convert_fusion.3
  95.0 0.1 exponential_multiply_fusion.1
  95.1 0.5 fusion.3
  95.6 1.8 fusion.41
  97.5 1.1 fusion.1
  98.6 0.2 multiply_reduce_fusion
  98.8 0.0 copy-done.7
  98.8 0.1 fusion.25
  98.9 30.6 %all-gather = bf16[8,4,512]{2,1,0:T(4,128)(2,1)S(1)} all-gather(bf16[1,4,512]{2,1,0:T(4,128)(2,1)S(1)} %reshape.79), channel_id=1, replica_groups=mesh['kv'=8,'tp'=4] {'kv'}, dimensions={0}, use_global_device_ids=true | all-gather | bytes 36864 | tf_op jit(solution)/shard_map/all_gather | solution.py:145
  129.5 1.2 convolution_convert_fusion.3
  130.7 10.3 %psum.35 = bf16[32,512]{1,0:T(8,128)(2,1)S(1)} all-reduce(bf16[32,512]{1,0:T(8,128)(2,1)S(1)} %convolution_convert_fusion.3), channel_id=1, replica_groups=mesh['kv'=8,'tp'=4] {'tp'}, use_global_device_ids=true, to_apply=%region_11.12 | all-reduce | flops 16384 | bytes 65536 | tf_op jit(solution)/shard_map/psum | solution.py:14
  141.0 0.0 copy-done.3
  141.0 0.0 copy-start.1
  141.0 0.1 fusion.14
  141.2 1.6 convolution_convert_fusion
  142.8 0.0 copy-done.1
  142.8 1.6 convolution_convert_fusion.1
  144.4 0.0 all-reduce.13.cloned.1.call-update
  144.4 20.6 %psum.37 = bf16[32]{0:T(256)(128)(2,1)S(1)} all-reduce(bf16[32]{0:T(256)(128)(2,1)S(1)} %get-tuple-element.11), channel_id=1, replica_groups=mesh['kv'=8,'tp'=4] {'kv'}, use_global_device_ids=true, to_apply=%region_14.15 | all-reduce | flops 32 | bytes 128 | tf_op jit(solution)/shard_map/psum | solution.py:159
  165.1 51.4 %all-reduce.13.cloned.1.call-done = (bf16[32,2752]{1,0:T(8,128)(2,1)}, bf16[32,2752]{1,0:T(8,128)(2,1)}) async-done(((bf16[32,2752]{1,0:T(8,128)(2,1)}, bf16[32,2752]{1,0:T(8,128)(2,1)}), (bf16[32,2752]{1,0:T(8,128)(2,1)}, bf16[32,2752]{1,0:T(8,128)(2,1)})) %all-reduce.13.cloned.1.call-update) | async-done | bytes 352272 | tf_op jit(solution)/shard_map/psum | solution.py:158
  216.4 2.6 %convolution_convert_fusion.2 = bf16[32,512]{1,0:T(8,128)(2,1)S(1)} fusion(bf16[2752,512]{1,0:T(8,128)(2,1)} %param.39, bf16[32,2752]{1,0:T(8,128)(2,1)} %get-tuple-element.9, bf16[32,2752]{1,0:T(8,128)(2,1)} %get-tuple-element.10, f32[32]{0:T(128)S(1)} %add_rsqrt_fusion.1), kind=kOutput, calls=%fused_computation.2 | convolution fusion | flops 91074560 | bytes 3203200 | tf_op jit(solution)/shard_map/dot_general | solution.py:162
  219.1 10.3 %psum.39 = bf16[32,512]{1,0:T(8,128)(2,1)S(1)} all-reduce(bf16[32,512]{1,0:T(8,128)(2,1)S(1)} %convolution_convert_fusion.2), channel_id=1, replica_groups=mesh['kv'=8,'tp'=4] {'tp'}, use_global_device_ids=true, to_apply=%region_16.17 | all-reduce | flops 16384 | bytes 65536 | tf_op jit(solution)/shard_map/psum | solution.py:14
  229.4 0.6 fusion.15
  (18 shorter events, 0.1 us)
Async XLA Ops:
  7.2 134.0 %copy-start = (bf16[512,2752]{0,1:T(8,128)(2,1)S(1)}, bf16[512,2752]{0,1:T(8,128)(2,1)}, u32[]{:S(2)}) copy-start(bf16[512,2752]{0,1:T(8,128)(2,1)} %param.38) | copy-start | bytes 8454148
  7.2 15.7 %copy-start.2 = (f32[4,64,2,128]{3,2,1,0:T(2,128)S(1)}, f32[4,64,2,128]{3,2,1,0:T(2,128)}, u32[]{:S(2)}) copy-start(f32[4,64,2,128]{3,2,1,0:T(2,128)} %param.32) | copy-start | bytes 786436
  7.2 85.3 %copy-start.9 = (f32[256]{0:T(256)S(1)}, f32[256]{0:T(256)}, u32[]{:S(2)}) copy-start(f32[256]{0:T(256)} %param.28) | copy-start | bytes 3076
  7.2 85.3 %copy-start.8 = (bf16[16,256]{1,0:T(8,128)(2,1)S(1)}, bf16[16,256]{1,0:T(8,128)(2,1)}, u32[]{:S(2)}) copy-start(bf16[16,256]{1,0:T(8,128)(2,1)} %param.27) | copy-start | bytes 24580
  7.2 91.5 %copy-start.7 = (f32[256]{0:T(256)S(1)}, f32[256]{0:T(256)}, u32[]{:S(2)}) copy-start(f32[256]{0:T(256)} %param.29) | copy-start | bytes 3076
  7.2 84.6 %all-reduce.11.cloned.1.call-start = ((), (), s32[]{:S(2)}) async-start(), calls=%async_computation | async-start | bytes 214016
  10.3 130.7 %copy-start.3 = (bf16[32,512]{1,0:T(8,128)(2,1)S(1)}, bf16[32,512]{1,0:T(8,128)(2,1)}, u32[]{:S(2)}) copy-start(bf16[32,512]{1,0:T(8,128)(2,1)} %param.20) | copy-start | bytes 98308
  12.0 129.1 %copy-start.6 = (f32[512]{0:T(512)S(1)}, f32[512]{0:T(512)}, u32[]{:S(2)}) copy-start(f32[512]{0:T(512)} %param.36) | copy-start | bytes 6148
  17.6 198.9 %all-reduce.13.cloned.1.call-start = ((), (), s32[]{:S(2)}) async-start(), calls=%async_computation.1 | async-start | bytes 720896 | tf_op jit(solution)/shard_map/psum | solution.py:158
  94.2 48.6 %copy-start.5 = (bf16[4,2,128]{2,1,0:T(2,128)(2,1)}, bf16[4,2,128]{2,1,0:T(2,128)(2,1)S(1)}, u32[]{:S(2)}) copy-start(bf16[4,2,128]{2,1,0:T(2,128)(2,1)S(1)} %reshape.74) | copy-start | bytes 6148
  95.0 47.8 %copy-start.4 = (bf16[4,2,256]{2,1,0:T(2,128)(2,1)}, bf16[4,2,256]{2,1,0:T(2,128)(2,1)S(1)}, u32[]{:S(2)}) copy-start(bf16[4,2,256]{2,1,0:T(2,128)(2,1)S(1)} %reshape.75) | copy-start | bytes 12292
  141.0 1.8 copy-start.1
Sparse Core Ops, SparseCore 0:
  17.7 74.0 all-reduce.10
  144.6 71.8 all-reduce.12
where the time goes:
time: 238 us; the launch traced here: 237 us
  waiting for transfers between devices  120 us (50%)
  blocking collectives  71.8 us (30%)
  matrix products  20.1 us (8%)
  between operations  14.8 us (6%)
  other arithmetic  8.62 us (4%)
    unnamed x3, waiting for transfers between devices  68.6 us
    psum x1, waiting for transfers between devices, on_device(): lax.psum(up_part.astype(jnp.bfloat16), 'kv').astype(jnp.float32)  51.4 us
    all_gather x1, blocking collectives, on_device(): lax.all_gather(heads_out, 'kv', axis=0, tiled=True)  30.6 us
    psum x1, blocking collectives, on_device(): lax.psum(mid_squares.astype(jnp.bfloat16), 'kv').astype(jnp.float32)  20.6 us
    psum x2, blocking collectives, across_heads(): lax.psum(partial_value.astype(jnp.bfloat16), 'tp').astype(jnp.float32)  20.5 us
  transfers between devices with their start and end apart: 2, of which 2 were waited for; matrix products, arithmetic and copies ran while one was open for 2% of the time, Pallas kernels for 0%

commit v1 on v0

v1 whole, which is shorter than its diff:
```python
import functools

import jax
import jax.numpy as jnp
from jax import lax
from jax.experimental import pallas as pl
from jax.experimental.pallas import tpu as pltpu
from jax.sharding import PartitionSpec as P

EPS = 1e-06
GATE_TEMP = 16.0
LANES = 128
F32 = jnp.float32
BF16 = jnp.bfloat16


def split_sum(column):
    high = column.astype(BF16).astype(F32)
    return high, column - high


def dot(left, right):
    return jnp.dot(left, right, preferred_element_type=F32)


def tiles_of(total, step):
    return [(start, min(step, total - start)) for start in range(0, total, step)]


def layer_kernel(
    n_kv,
    n_tp,
    width,
    tokens_h,
    attn_gain_h,
    wq_h,
    wk_h,
    wv_h,
    wg_h,
    wc_h,
    dw_h,
    db_h,
    head_gain_h,
    key_h,
    value_h,
    decay_h,
    state_h,
    lengths_s,
    wo_h,
    mlp_gain_h,
    gate_h,
    up_h,
    down_h,
    out_ref,
    nk_ref,
    nv_ref,
    tokens,
    attn_gain,
    wq,
    wk,
    wv,
    wg,
    wc,
    dw,
    db,
    head_gain,
    key,
    value,
    decay,
    state,
    wo,
    mlp_gain,
    gate,
    up,
    down,
    proj,
    proj_send,
    proj_recv,
    keyed,
    total_exp,
    decayed3,
    keys3,
    values3,
    mixed,
    heads,
    heads_all,
    attended,
    mlp_acc,
    mlp_send,
    mlp_recv,
    hidden,
    hidden_all,
    lifted,
    load_sem,
    send_a,
    recv_a,
    send_b,
    recv_b,
    send_c,
    recv_c,
    send_d,
    recv_d,
    send_e,
    recv_e,
    send_f,
    recv_f,
):
    kv_me = lax.axis_index("kv")
    tp_me = lax.axis_index("tp")
    rows, feats = tokens.shape
    seqs, span, heads_here, key_dim = key.shape
    value_dim = value.shape[3]
    kw, vw = heads_here * key_dim, heads_here * value_dim
    rank = wc.shape[1]
    units = gate.shape[1]
    padded = hidden.shape[1]

    loads = {}
    pairs = [
        ("tokens", tokens_h, tokens),
        ("attn_gain", attn_gain_h, attn_gain),
        ("wc", wc_h, wc),
        ("wq", wq_h, wq),
        ("wk", wk_h, wk),
        ("wv", wv_h, wv),
        ("wg", wg_h, wg),
        ("decay", decay_h, decay),
        ("key", key_h, key),
        ("dw", dw_h, dw.at[pl.ds(0, rank)]),
        ("db", db_h, db),
        ("head_gain", head_gain_h, head_gain),
        ("state", state_h, state),
        ("value", value_h, value),
        ("wo", wo_h, wo),
        ("mlp_gain", mlp_gain_h, mlp_gain),
        ("gate", gate_h, gate),
        ("up", up_h, up),
        ("down", down_h, down.at[pl.ds(0, units)]),
    ]
    for place, (name, source, target) in enumerate(pairs):
        loads[name] = pltpu.make_async_copy(source, target, load_sem.at[place])
        loads[name].start()

    barrier = pltpu.get_barrier_semaphore()
    for off in range(1, n_kv):
        pl.semaphore_signal(
            barrier,
            inc=1,
            device_id={"kv": lax.rem(kv_me + off, n_kv)},
            device_id_type=pl.DeviceIdType.MESH,
        )
    for off in range(1, n_tp):
        pl.semaphore_signal(
            barrier,
            inc=1,
            device_id={"tp": lax.rem(tp_me + off, n_tp)},
            device_id_type=pl.DeviceIdType.MESH,
        )

    def exchange(axis, me, count, source, target, sends, recvs):
        started = []
        for off in range(count - 1, 0, -1):
            p = lax.rem(me + off, count)
            copy = pltpu.make_async_remote_copy(
                src_ref=source(p),
                dst_ref=target.at[me],
                send_sem=sends.at[off],
                recv_sem=recvs.at[me],
                device_id={axis: p},
                device_id_type=pl.DeviceIdType.MESH,
            )
            copy.start()
            started.append(copy)
        return started

    def await_arrivals(me, count, target, recvs):
        for off in range(1, count):
            p = lax.rem(me + off, count)
            pltpu.make_async_copy(target.at[p], target.at[p], recvs.at[p]).wait()

    pending = []

    base_misc = 2 * kw + 2 * vw
    for name in ("tokens", "attn_gain", "wc"):
        loads[name].wait()
    token_f = tokens[...].astype(F32)
    scaled = (token_f * attn_gain[...]).astype(BF16)
    proj[:, base_misc:] = jnp.zeros((rows, LANES), F32)
    proj[:, base_misc : base_misc + rank] = dot(scaled, wc[...])
    high, low = split_sum(jnp.sum(token_f * token_f, axis=1, keepdims=True))
    proj[:, base_misc + rank : base_misc + rank + 1] = high
    proj[:, base_misc + rank + 1 : base_misc + rank + 2] = low
    base = 0
    for name, weight in (("wq", wq), ("wk", wk), ("wv", wv), ("wg", wg)):
        loads[name].wait()
        for start, size in tiles_of(weight.shape[1], 256):
            proj[:, base + start : base + start + size] = dot(
                scaled, weight[:, start : start + size]
            )
        base += weight.shape[1]
    for p in range(n_kv):
        proj_send[p] = proj[p * seqs : (p + 1) * seqs, :].astype(BF16)
    pl.semaphore_wait(barrier, n_kv + n_tp - 2)
    pending += exchange("kv", kv_me, n_kv, lambda p: proj_send.at[p], proj_recv, send_a, recv_a)
    proj_recv[kv_me] = proj_send[kv_me]

    dw[rank:, :] = jnp.zeros((dw.shape[0] - rank, dw.shape[1]), BF16)
    if padded > units:
        down[units:, :] = jnp.zeros((padded - units, down.shape[1]), BF16)
        hidden[:, units:] = jnp.zeros((rows, padded - units), F32)
    loads["decay"].wait()
    loads["key"].wait()
    positions = lax.broadcasted_iota(jnp.int32, (span, heads_here, key_dim), 0)
    for b in range(seqs):
        live = positions < lengths_s[b]
        kept = jnp.where(live, decay[b], 0.0)
        suffix = kept
        step = 1
        while step < span:
            suffix = suffix + jnp.concatenate(
                [suffix[step:], jnp.zeros((step, heads_here, key_dim), F32)], axis=0
            )
            step *= 2
        total_exp[b] = jnp.exp(suffix[0])
        later = jnp.concatenate([suffix[1:], jnp.zeros((1, heads_here, key_dim), F32)], axis=0)
        keyed[b] = jnp.where(live, key[b].astype(F32) * jnp.exp(later), 0.0)
    for name in ("dw", "db", "head_gain", "state", "value"):
        loads[name].wait()

    await_arrivals(kv_me, n_kv, proj_recv, recv_a)
    total = proj_recv[0].astype(F32)
    for p in range(1, n_kv):
        total = total + proj_recv[p].astype(F32)
    misc = total[:, base_misc:]
    squares = misc[:, rank : rank + 1] + misc[:, rank + 1 : rank + 2]
    inv_rms = lax.rsqrt(squares / width + EPS)
    queries = (total[:, :kw] * inv_rms * key_dim ** (-0.5)).astype(BF16).astype(F32)
    new_keys = (total[:, kw : 2 * kw] * inv_rms).astype(BF16).astype(F32)
    new_values = (total[:, 2 * kw : 2 * kw + vw] * inv_rms).astype(BF16).astype(F32)
    out_gate = (total[:, 2 * kw + vw : base_misc] * inv_rms).astype(BF16).astype(F32)
    code = (misc * inv_rms).astype(BF16)
    pre_gate = dot(code, dw[...]) + db[...]
    new_decay = (jnp.minimum(pre_gate, 0.0) - jnp.log1p(jnp.exp(-jnp.abs(pre_gate)))) / GATE_TEMP
    decayed = queries * jnp.exp(new_decay)
    for b in range(seqs):
        for h in range(heads_here):
            k_cols = slice(h * key_dim, (h + 1) * key_dim)
            v_cols = slice(h * value_dim, (h + 1) * value_dim)
            decayed3[b, h : h + 1, :] = decayed[b : b + 1, k_cols]
            keys3[b, h : h + 1, :] = new_keys[b : b + 1, k_cols]
            values3[b, h : h + 1, :] = new_values[b : b + 1, v_cols]
    nk_ref[...] = keys3[...].astype(BF16)
    nv_ref[...] = values3[...].astype(BF16)
    for b in range(seqs):
        d = decayed3[b]
        scores = jnp.sum(keyed[b] * d[None], axis=-1, keepdims=True)
        scores = scores.astype(BF16).astype(F32)
        within = jnp.sum(scores * value[b].astype(F32), axis=0)
        into_state = jnp.transpose(
            jnp.concatenate(
                [d * total_exp[b], jnp.zeros((8 - heads_here, key_dim), F32)], axis=0
            )
        )
        for h in range(heads_here):
            carried = jnp.sum(into_state[:, h : h + 1] * state[b, h], axis=0, keepdims=True)
            mixed[b : b + 1, h * value_dim : (h + 1) * value_dim] = carried + within[h : h + 1]
    for h in range(heads_here):
        k_cols = slice(h * key_dim, (h + 1) * key_dim)
        v_cols = slice(h * value_dim, (h + 1) * value_dim)
        own = jnp.sum(queries[:, k_cols] * new_keys[:, k_cols], axis=-1, keepdims=True)
        full = mixed[:, v_cols] + own * new_values[:, v_cols]
        norm = lax.rsqrt(jnp.mean(full * full, axis=-1, keepdims=True) + EPS)
        g = out_gate[:, v_cols]
        mixed[:, v_cols] = full * norm * head_gain[...] * (g / (1.0 + jnp.exp(-g)))
    heads_all[kv_me] = mixed[...].astype(BF16)
    pending += exchange(
        "kv", kv_me, n_kv, lambda p: heads_all.at[kv_me], heads_all, send_b, recv_b
    )

    loads["wo"].wait()
    loads["mlp_gain"].wait()
    await_arrivals(kv_me, n_kv, heads_all, recv_b)
    for p in range(n_kv):
        heads[p * seqs : (p + 1) * seqs, :] = heads_all[p].astype(F32)
    attended[tp_me] = dot(heads[...].astype(BF16), wo[...]).astype(BF16)
    pending += exchange(
        "tp", tp_me, n_tp, lambda p: attended.at[tp_me], attended, send_c, recv_c
    )
    loads["gate"].wait()
    await_arrivals(tp_me, n_tp, attended, recv_c)
    summed = attended[0].astype(F32)
    for p in range(1, n_tp):
        summed = summed + attended[p].astype(F32)
    mid_f = (token_f + summed).astype(BF16).astype(F32)
    scaled_mid = (mid_f * mlp_gain[...]).astype(BF16)

    for part, (name, weight) in enumerate((("gate", gate), ("up", up))):
        if part:
            loads[name].wait()
        else:
            mlp_acc[:, padded - LANES :] = jnp.zeros((rows, LANES), F32)
        for start, size in tiles_of(units, 256):
            mlp_acc[:, start : start + size] = dot(scaled_mid, weight[:, start : start + size])
        if part == 0:
            high, low = split_sum(jnp.sum(mid_f * mid_f, axis=1, keepdims=True))
            mlp_acc[:, units : units + 1] = high
            mlp_acc[:, units + 1 : units + 2] = low
        for p in range(n_kv):
            mlp_send[part, p] = mlp_acc[p * seqs : (p + 1) * seqs, :].astype(BF16)
        pending += exchange(
            "kv",
            kv_me,
            n_kv,
            lambda p, part=part: mlp_send.at[part, p],
            mlp_recv.at[part],
            send_d.at[part],
            recv_d.at[part],
        )
        mlp_recv[part, kv_me] = mlp_send[part, kv_me]
    sums = []
    for part in range(2):
        await_arrivals(kv_me, n_kv, mlp_recv.at[part], recv_d.at[part])
        total = mlp_recv[part, 0].astype(F32)
        for p in range(1, n_kv):
            total = total + mlp_recv[part, p].astype(F32)
        sums.append(total)
    squares = sums[0][:, units : units + 1] + sums[0][:, units + 1 : units + 2]
    inv_mid = lax.rsqrt(squares / width + EPS)
    g = sums[0] * inv_mid
    mine = g / (1.0 + jnp.exp(-g)) * (sums[1] * inv_mid)
    hidden_all[kv_me] = mine.astype(BF16)
    pending += exchange(
        "kv", kv_me, n_kv, lambda p: hidden_all.at[kv_me], hidden_all, send_e, recv_e
    )
    loads["down"].wait()
    await_arrivals(kv_me, n_kv, hidden_all, recv_e)
    for p in range(n_kv):
        hidden[p * seqs : (p + 1) * seqs, :units] = hidden_all[p].astype(F32)[:, :units]
    acc = jnp.zeros((rows, feats), F32)
    for start, size in tiles_of(padded, 256):
        acc = acc + dot(hidden[:, start : start + size].astype(BF16), down[start : start + size, :])
    lifted[tp_me] = acc.astype(BF16)
    pending += exchange("tp", tp_me, n_tp, lambda p: lifted.at[tp_me], lifted, send_f, recv_f)
    await_arrivals(tp_me, n_tp, lifted, recv_f)
    summed = lifted[0].astype(F32)
    for p in range(1, n_tp):
        summed = summed + lifted[p].astype(F32)
    out_ref[...] = (mid_f + summed).astype(BF16)
    for copy in pending:
        copy.wait_send()


def on_device(n_kv, n_tp, *args):
    (
        tokens,
        attn_gain,
        wq,
        wk,
        wv,
        wg,
        wc,
        dw,
        db,
        head_gain,
        key,
        value,
        decay,
        state,
        lengths,
        wo,
        mlp_gain,
        gate,
        up,
        down,
    ) = args
    row = lambda a: a.reshape(1, a.shape[0])
    operands = [
        tokens,
        row(attn_gain),
        wq,
        wk,
        wv,
        wg,
        wc,
        dw,
        row(db),
        row(head_gain),
        key,
        value,
        decay,
        state,
        lengths,
        wo,
        row(mlp_gain),
        gate,
        up,
        down,
    ]
    rows, feats = tokens.shape
    seqs, span, heads_here, key_dim = key.shape
    value_dim = value.shape[3]
    kw, vw = heads_here * key_dim, heads_here * value_dim
    units = gate.shape[1]
    rank = wc.shape[1]
    padded = (units + 2 + LANES - 1) // LANES * LANES
    cols = 2 * kw + 2 * vw + LANES
    vmem = pltpu.VMEM

    def copied(a):
        if a is lengths:
            return None
        if a is dw:
            return vmem((LANES, a.shape[1]), a.dtype)
        if a is down:
            return vmem((padded, a.shape[1]), a.dtype)
        return vmem(a.shape, a.dtype)

    scratch = [c for c in map(copied, operands) if c is not None]
    scratch += [
        vmem((rows, cols), F32),
        vmem((n_kv, seqs, cols), BF16),
        vmem((n_kv, seqs, cols), BF16),
        vmem((seqs, span, heads_here, key_dim), F32),
        vmem((seqs, heads_here, key_dim), F32),
        vmem((seqs, heads_here, key_dim), F32),
        vmem((seqs, heads_here, key_dim), F32),
        vmem((seqs, heads_here, value_dim), F32),
        vmem((seqs, vw), F32),
        vmem((rows, vw), F32),
        vmem((n_kv, seqs, vw), BF16),
        vmem((n_tp, rows, feats), BF16),
        vmem((rows, padded), F32),
        vmem((2, n_kv, seqs, padded), BF16),
        vmem((2, n_kv, seqs, padded), BF16),
        vmem((rows, padded), F32),
        vmem((n_kv, seqs, padded), BF16),
        vmem((n_tp, rows, feats), BF16),
    ]
    dma = pltpu.SemaphoreType.DMA
    scratch += [dma((19,))]
    scratch += [dma((n_kv,))] * 4
    scratch += [dma((n_tp,))] * 2
    scratch += [dma((2, n_kv))] * 2
    scratch += [dma((n_kv,))] * 2
    scratch += [dma((n_tp,))] * 2
    any_spec = pl.BlockSpec(memory_space=pl.ANY)
    in_specs = [
        pl.BlockSpec(memory_space=pltpu.SMEM) if a is lengths else any_spec for a in operands
    ]
    return pl.pallas_call(
        functools.partial(layer_kernel, n_kv, n_tp, feats * n_kv),
        out_shape=(
            jax.ShapeDtypeStruct((rows, feats), BF16),
            jax.ShapeDtypeStruct((seqs, heads_here, key_dim), BF16),
            jax.ShapeDtypeStruct((seqs, heads_here, value_dim), BF16),
        ),
        in_specs=in_specs,
        out_specs=(pl.BlockSpec(memory_space=pltpu.VMEM),) * 3,
        scratch_shapes=scratch,
        compiler_params=pltpu.CompilerParams(
            collective_id=0, has_side_effects=True, vmem_limit_bytes=60 * 1024 * 1024
        ),
        name="layer",
    )(*operands)


def solution(mesh):
    in_specs = (
        P(None, "kv"),
        P("kv"),
        P("kv", "tp"),
        P("kv", "tp"),
        P("kv", "tp"),
        P("kv", "tp"),
        P("kv", None),
        P(None, "tp"),
        P("tp"),
        P(),
        P("kv", None, "tp", None),
        P("kv", None, "tp", None),
        P("kv", None, "tp", None),
        P("kv", "tp", None, None),
        P("kv"),
        P("tp", "kv"),
        P("kv"),
        P("kv", "tp"),
        P("kv", "tp"),
        P("tp", "kv"),
    )
    out_specs = (P(None, "kv"), P("kv", "tp", None), P("kv", "tp", None))
    return jax.shard_map(
        functools.partial(on_device, mesh.shape["kv"], mesh.shape["tp"]),
        mesh=mesh,
        in_specs=in_specs,
        out_specs=out_specs,
        check_vma=False,
    )
```

time: 238 us -> 54.7 us (0.23)
  waiting for transfers between devices: 120 us -> 0 us
  blocking collectives: 71.8 us -> 0 us
  Pallas kernels: 0 us -> 40.7 us
  matrix products: 20.1 us -> 0 us
  between operations: 14.8 us -> 0.64 us
  local copies, waits for them, and re-layouts: 1.43 us -> 13 us
  other arithmetic: 8.62 us -> 0 us
    unnamed x3 -> x0, waiting for transfers between devices: 68.6 us -> none
    psum x1 -> x0, waiting for transfers between devices: 51.4 us -> none  [on_device(): lax.psum(up_part.astype(jnp.bfloat16), 'kv').astype(jnp.float32)]
    psum x3 -> x0, blocking collectives: 41.2 us -> none  [the longest x1 20.6 us: on_device(): lax.psum(mid_squares.astype(jnp.bfloat16), 'kv').astype(jnp.float32)]
    pallas_call x0 -> x1, Pallas kernels: none -> 40.7 us  [on_device(): pl.pallas_call(functools.partial(layer_kernel, n_kv, n_tp, feats * n_kv),...]
    all_gather x1 -> x0, blocking collectives: 30.6 us -> none  [on_device(): lax.all_gather(heads_out, 'kv', axis=0, tiled=True)]
    dot_general x13 -> x0, matrix products: 20.1 us -> none  [the longest x1 2.64 us: on_device(): jnp.dot(hidden, down_weight, preferred_element_type=jnp.float32)]
    unnamed x23 -> x8, local copies, waits for them, and re-layouts: 1.36 us -> 13 us
    another operation x1 -> x0, other arithmetic: 2.61 us -> none  [block_attention(): later_sum = lax.cumsum(kept_decay, axis=1, reverse=True) - kept_decay]
  transfers between devices with their start and end apart: 2 -> 0, of which waited for: 2 -> 0; matrix products, arithmetic and copies ran while one was open for 2% -> 0% of each run, Pallas kernels for 0% -> 0%
where the time goes in v1:
time: 54.7 us; the launch traced here: 54.4 us
  Pallas kernels  40.7 us (74%)
  local copies, waits for them, and re-layouts  13 us (24%)
  between operations  0.64 us (1%)
    pallas_call x1, Pallas kernels, on_device(): pl.pallas_call(functools.partial(layer_kernel, n_kv, n_tp, feats * n_kv),...  40.7 us
    unnamed x8, local copies, waits for them, and re-layouts  13 us

profile of v1, /device:TPU:0, one launch (start us, length us, event | category | flops | bytes accessed | tf_op | source)
XLA Modules:
  0.0 54.4 jit_solution(16202518634397932874)
XLA Ops:
  0.6 1.5 %copy.23.wc_h = bf16[512,16]{1,0:T(8,128)(2,1)} copy(bf16[512,16]{0,1:T(8,128)(2,1)} %param.26) | data formatting | bytes 32768 | tf_op args[6]
  2.1 0.0 copy-start
  2.1 4.7 %copy.24.gate_h = bf16[512,2752]{1,0:T(8,128)(2,1)} copy(bf16[512,2752]{0,1:T(8,128)(2,1)} %param.37) | data formatting | bytes 5636096 | tf_op args[17]
  6.8 0.0 copy-done
  6.8 3.0 %copy.25.up_h = bf16[512,2752]{1,0:T(8,128)(2,1)} copy(bf16[512,2752]{0,1:T(8,128)(2,1)S(1)} %copy-done) | data formatting | bytes 5636096 | tf_op args[18]
  9.8 40.7 %layer.1 = (bf16[32,512]{1,0:T(8,128)(2,1)}, bf16[4,2,128]{2,1,0:T(2,128)(2,1)}, bf16[4,2,256]{2,1,0:T(2,128)(2,1)}) custom-call(bf16[32,512]{1,0:T(8,128)(2,1)} %tokens_h.1, f32[1,512]{1,0:T(1,128)} %bitcast.4, bf16[512,256]{1,0:T(8,128)(2,1)} %wq_h.1, bf16[512,256]{1,0:T(8,128)(2,1)} %wk_h.1, bf16[512,512]{1,0:T(8,128)(2,1)} %wv_h.1, ...), custom_call_target="tpu_custom_call" | custom-call | tf_op jit(solution)/shard_map/layer/pallas_call | solution.py:450
  50.5 1.4 %copy.29 = bf16[32,512]{1,0:T(8,128)(2,1)} copy(bf16[32,512]{1,0:T(8,128)(2,1)} %get-tuple-element.6) | data formatting | bytes 65536
  51.9 1.2 %copy.30 = bf16[4,2,128]{2,1,0:T(2,128)(2,1)} copy(bf16[4,2,128]{2,1,0:T(2,128)(2,1)} %get-tuple-element.7) | data formatting | bytes 4096
  53.1 1.3 %copy.31 = bf16[4,2,256]{2,1,0:T(2,128)(2,1)} copy(bf16[4,2,256]{2,1,0:T(2,128)(2,1)} %get-tuple-element.8) | data formatting | bytes 8192
Async XLA Ops:
  2.1 4.7 %copy-start = (bf16[512,2752]{0,1:T(8,128)(2,1)S(1)}, bf16[512,2752]{0,1:T(8,128)(2,1)}, u32[]{:S(2)}) copy-start(bf16[512,2752]{0,1:T(8,128)(2,1)} %param.38) | copy-start | bytes 8454148

commit v2 on v1

--- a/solution.py
+++ b/solution.py
@@ -9,6 +9,8 @@
 
 EPS = 1e-06
 GATE_TEMP = 16.0
+FIRST_LOADS = 7
+PARTS = 4
 LANES = 128
 F32 = jnp.float32
 BF16 = jnp.bfloat16
@@ -23,8 +25,31 @@
     return jnp.dot(left, right, preferred_element_type=F32)
 
 
+def dot_t(left, right):
+    return lax.dot_general(left, right, (((1,), (1,)), ((), ())), preferred_element_type=F32)
+
+
 def tiles_of(total, step):
     return [(start, min(step, total - start)) for start in range(0, total, step)]
+
+
+def pieces_of(units):
+    each = units // PARTS // LANES * LANES
+    head = units - (PARTS - 1) * each
+    room = (head + 2 + LANES - 1) // LANES * LANES
+    return [(0, head, room)] + [(head + k * each, each, each) for k in range(PARTS - 1)]
+
+
+def copy_out(*refs):
+    *arrays, sems = refs
+    half = len(arrays) // 2
+    copies = [
+        pltpu.make_async_copy(arrays[k], arrays[half + k], sems.at[k]) for k in range(half)
+    ]
+    for copy in copies:
+        copy.start()
+    for copy in copies:
+        copy.wait()
 
 
 def layer_kernel(
@@ -85,11 +110,11 @@
     heads,
     heads_all,
     attended,
-    mlp_acc,
-    mlp_send,
-    mlp_recv,
-    hidden,
-    hidden_all,
+    accs,
+    sends,
+    recvs,
+    hiddens,
+    hiddens_all,
     lifted,
     load_sem,
     send_a,
@@ -111,9 +136,9 @@
     seqs, span, heads_here, key_dim = key.shape
     value_dim = value.shape[3]
     kw, vw = heads_here * key_dim, heads_here * value_dim
-    rank = wc.shape[1]
-    units = gate.shape[1]
-    padded = hidden.shape[1]
+    rank = wc.shape[0]
+    units = gate.shape[0]
+    pieces = pieces_of(units)
 
     loads = {}
     pairs = [
@@ -135,11 +160,16 @@
         ("mlp_gain", mlp_gain_h, mlp_gain),
         ("gate", gate_h, gate),
         ("up", up_h, up),
-        ("down", down_h, down.at[pl.ds(0, units)]),
+        ("down", down_h, down),
     ]
     for place, (name, source, target) in enumerate(pairs):
         loads[name] = pltpu.make_async_copy(source, target, load_sem.at[place])
-        loads[name].start()
+        if place < FIRST_LOADS:
+            loads[name].start()
+
+    def ready(*names):
+        for name in names:
+            loads.pop(name).wait()
 
     barrier = pltpu.get_barrier_semaphore()
     for off in range(1, n_kv):
@@ -157,15 +187,15 @@
             device_id_type=pl.DeviceIdType.MESH,
         )
 
-    def exchange(axis, me, count, source, target, sends, recvs):
+    def exchange(axis, me, count, source, target, sent, arrived):
         started = []
         for off in range(count - 1, 0, -1):
             p = lax.rem(me + off, count)
             copy = pltpu.make_async_remote_copy(
                 src_ref=source(p),
                 dst_ref=target.at[me],
-                send_sem=sends.at[off],
-                recv_sem=recvs.at[me],
+                send_sem=sent.at[off],
+                recv_sem=arrived.at[me],
                 device_id={axis: p},
                 device_id_type=pl.DeviceIdType.MESH,
             )
@@ -173,26 +203,28 @@
             started.append(copy)
         return started
 
-    def await_arrivals(me, count, target, recvs):
+    def await_arrivals(me, count, target, arrived):
         for off in range(1, count):
             p = lax.rem(me + off, count)
-            pltpu.make_async_copy(target.at[p], target.at[p], recvs.at[p]).wait()
+            pltpu.make_async_copy(target.at[p], target.at[p], arrived.at[p]).wait()
 
     pending = []
 
     base_misc = 2 * kw + 2 * vw
-    for name in ("tokens", "attn_gain", "wc"):
-        loads[name].wait()
+    ready(*("tokens", "attn_gain", "wc"))
     token_f = tokens[...].astype(F32)
     scaled = (token_f * attn_gain[...]).astype(BF16)
     proj[:, base_misc:] = jnp.zeros((rows, LANES), F32)
-    proj[:, base_misc : base_misc + rank] = dot(scaled, wc[...])
+    proj[:, base_misc : base_misc + rank] = dot_t(scaled, wc[...])
     high, low = split_sum(jnp.sum(token_f * token_f, axis=1, keepdims=True))
     proj[:, base_misc + rank : base_misc + rank + 1] = high
     proj[:, base_misc + rank + 1 : base_misc + rank + 2] = low
     base = 0
     for name, weight in (("wq", wq), ("wk", wk), ("wv", wv), ("wg", wg)):
-        loads[name].wait()
+        ready(name)
+        if name == "wg":
+            for late in list(loads.values()):
+                late.start()
         for start, size in tiles_of(weight.shape[1], 256):
             proj[:, base + start : base + start + size] = dot(
                 scaled, weight[:, start : start + size]
@@ -205,11 +237,8 @@
     proj_recv[kv_me] = proj_send[kv_me]
 
     dw[rank:, :] = jnp.zeros((dw.shape[0] - rank, dw.shape[1]), BF16)
-    if padded > units:
-        down[units:, :] = jnp.zeros((padded - units, down.shape[1]), BF16)
-        hidden[:, units:] = jnp.zeros((rows, padded - units), F32)
-    loads["decay"].wait()
-    loads["key"].wait()
+    ready("decay")
+    ready("key")
     positions = lax.broadcasted_iota(jnp.int32, (span, heads_here, key_dim), 0)
     for b in range(seqs):
         live = positions < lengths_s[b]
@@ -224,8 +253,7 @@
         total_exp[b] = jnp.exp(suffix[0])
         later = jnp.concatenate([suffix[1:], jnp.zeros((1, heads_here, key_dim), F32)], axis=0)
         keyed[b] = jnp.where(live, key[b].astype(F32) * jnp.exp(later), 0.0)
-    for name in ("dw", "db", "head_gain", "state", "value"):
-        loads[name].wait()
+    ready(*("dw", "db", "head_gain", "state", "value"))
 
     await_arrivals(kv_me, n_kv, proj_recv, recv_a)
     total = proj_recv[0].astype(F32)
@@ -277,8 +305,8 @@
         "kv", kv_me, n_kv, lambda p: heads_all.at[kv_me], heads_all, send_b, recv_b
     )
 
-    loads["wo"].wait()
-    loads["mlp_gain"].wait()
+    ready("wo")
+    ready("mlp_gain")
     await_arrivals(kv_me, n_kv, heads_all, recv_b)
     for p in range(n_kv):
         heads[p * seqs : (p + 1) * seqs, :] = heads_all[p].astype(F32)
@@ -286,7 +314,7 @@
     pending += exchange(
         "tp", tp_me, n_tp, lambda p: attended.at[tp_me], attended, send_c, recv_c
     )
-    loads["gate"].wait()
+    ready("gate")
     await_arrivals(tp_me, n_tp, attended, recv_c)
     summed = attended[0].astype(F32)
     for p in range(1, n_tp):
@@ -294,51 +322,67 @@
     mid_f = (token_f + summed).astype(BF16).astype(F32)
     scaled_mid = (mid_f * mlp_gain[...]).astype(BF16)
 
-    for part, (name, weight) in enumerate((("gate", gate), ("up", up))):
-        if part:
-            loads[name].wait()
-        else:
-            mlp_acc[:, padded - LANES :] = jnp.zeros((rows, LANES), F32)
-        for start, size in tiles_of(units, 256):
-            mlp_acc[:, start : start + size] = dot(scaled_mid, weight[:, start : start + size])
+    ready("up")
+    for part, (first, size, span_cols) in enumerate(pieces):
+        mlp_acc = accs[part]
+        for base, weight in ((0, gate), (span_cols, up)):
+            if size < span_cols:
+                mlp_acc[:, base + span_cols - LANES : base + span_cols] = jnp.zeros(
+                    (rows, LANES), F32
+                )
+            for start, count in tiles_of(size, 256):
+                mlp_acc[:, base + start : base + start + count] = dot_t(
+                    scaled_mid, weight[first + start : first + start + count, :]
+                )
         if part == 0:
             high, low = split_sum(jnp.sum(mid_f * mid_f, axis=1, keepdims=True))
-            mlp_acc[:, units : units + 1] = high
-            mlp_acc[:, units + 1 : units + 2] = low
+            mlp_acc[:, size : size + 1] = high
+            mlp_acc[:, size + 1 : size + 2] = low
         for p in range(n_kv):
-            mlp_send[part, p] = mlp_acc[p * seqs : (p + 1) * seqs, :].astype(BF16)
+            sends[part][p] = mlp_acc[p * seqs : (p + 1) * seqs, :].astype(BF16)
         pending += exchange(
             "kv",
             kv_me,
             n_kv,
-            lambda p, part=part: mlp_send.at[part, p],
-            mlp_recv.at[part],
+            lambda p, part=part: sends[part].at[p],
+            recvs[part],
             send_d.at[part],
             recv_d.at[part],
         )
-        mlp_recv[part, kv_me] = mlp_send[part, kv_me]
-    sums = []
-    for part in range(2):
-        await_arrivals(kv_me, n_kv, mlp_recv.at[part], recv_d.at[part])
-        total = mlp_recv[part, 0].astype(F32)
+        recvs[part][kv_me] = sends[part][kv_me]
+    for part, (first, size, span_cols) in enumerate(pieces):
+        await_arrivals(kv_me, n_kv, recvs[part], recv_d.at[part])
+        total = recvs[part][0].astype(F32)
         for p in range(1, n_kv):
-            total = total + mlp_recv[part, p].astype(F32)
-        sums.append(total)
-    squares = sums[0][:, units : units + 1] + sums[0][:, units + 1 : units + 2]
-    inv_mid = lax.rsqrt(squares / width + EPS)
-    g = sums[0] * inv_mid
-    mine = g / (1.0 + jnp.exp(-g)) * (sums[1] * inv_mid)
-    hidden_all[kv_me] = mine.astype(BF16)
-    pending += exchange(
-        "kv", kv_me, n_kv, lambda p: hidden_all.at[kv_me], hidden_all, send_e, recv_e
-    )
-    loads["down"].wait()
-    await_arrivals(kv_me, n_kv, hidden_all, recv_e)
-    for p in range(n_kv):
-        hidden[p * seqs : (p + 1) * seqs, :units] = hidden_all[p].astype(F32)[:, :units]
+            total = total + recvs[part][p].astype(F32)
+        if part == 0:
+            squares = total[:, size : size + 1] + total[:, size + 1 : size + 2]
+            inv_mid = lax.rsqrt(squares / width + EPS)
+        g = total[:, :span_cols] * inv_mid
+        mine = g / (1.0 + jnp.exp(-g)) * (total[:, span_cols:] * inv_mid)
+        hiddens_all[part][kv_me] = mine.astype(BF16)
+        pending += exchange(
+            "kv",
+            kv_me,
+            n_kv,
+            lambda p, part=part: hiddens_all[part].at[kv_me],
+            hiddens_all[part],
+            send_e.at[part],
+            recv_e.at[part],
+        )
+    ready("down")
     acc = jnp.zeros((rows, feats), F32)
-    for start, size in tiles_of(padded, 256):
-        acc = acc + dot(hidden[:, start : start + size].astype(BF16), down[start : start + size, :])
+    for part, (first, size, span_cols) in enumerate(pieces):
+        await_arrivals(kv_me, n_kv, hiddens_all[part], recv_e.at[part])
+        hidden = hiddens[part]
+        for p in range(n_kv):
+            hidden[p * seqs : (p + 1) * seqs, :] = hiddens_all[part][p].astype(F32)
+        if size < span_cols:
+            lane = lax.broadcasted_iota(jnp.int32, (rows, span_cols), 1)
+            whole = jnp.where(lane < size, hidden[...], 0.0).astype(BF16)
+        else:
+            whole = hidden[...].astype(BF16)
+        acc = acc + dot(whole, down[first : first + span_cols, :])
     lifted[tp_me] = acc.astype(BF16)
     pending += exchange("tp", tp_me, n_tp, lambda p: lifted.at[tp_me], lifted, send_f, recv_f)
     await_arrivals(tp_me, n_tp, lifted, recv_f)
@@ -381,7 +425,7 @@
         wk,
         wv,
         wg,
-        wc,
+        wc.T,
         dw,
         row(db),
         row(head_gain),
@@ -392,8 +436,8 @@
         lengths,
         wo,
         row(mlp_gain),
-        gate,
-        up,
+        gate.T,
+        up.T,
         down,
     ]
     rows, feats = tokens.shape
@@ -402,7 +446,7 @@
     kw, vw = heads_here * key_dim, heads_here * value_dim
     units = gate.shape[1]
     rank = wc.shape[1]
-    padded = (units + 2 + LANES - 1) // LANES * LANES
+    widths = [piece[2] for piece in pieces_of(units)]
     cols = 2 * kw + 2 * vw + LANES
     vmem = pltpu.VMEM
 
@@ -411,8 +455,6 @@
             return None
         if a is dw:
             return vmem((LANES, a.shape[1]), a.dtype)
-        if a is down:
-            return vmem((padded, a.shape[1]), a.dtype)
         return vmem(a.shape, a.dtype)
 
     scratch = [c for c in map(copied, operands) if c is not None]
@@ -429,39 +471,44 @@
         vmem((rows, vw), F32),
         vmem((n_kv, seqs, vw), BF16),
         vmem((n_tp, rows, feats), BF16),
-        vmem((rows, padded), F32),
-        vmem((2, n_kv, seqs, padded), BF16),
-        vmem((2, n_kv, seqs, padded), BF16),
-        vmem((rows, padded), F32),
-        vmem((n_kv, seqs, padded), BF16),
+        [vmem((rows, 2 * w), F32) for w in widths],
+        [vmem((n_kv, seqs, 2 * w), BF16) for w in widths],
+        [vmem((n_kv, seqs, 2 * w), BF16) for w in widths],
+        [vmem((rows, w), F32) for w in widths],
+        [vmem((n_kv, seqs, w), BF16) for w in widths],
         vmem((n_tp, rows, feats), BF16),
     ]
     dma = pltpu.SemaphoreType.DMA
     scratch += [dma((19,))]
     scratch += [dma((n_kv,))] * 4
     scratch += [dma((n_tp,))] * 2
-    scratch += [dma((2, n_kv))] * 2
-    scratch += [dma((n_kv,))] * 2
+    scratch += [dma((PARTS, n_kv))] * 4
     scratch += [dma((n_tp,))] * 2
-    any_spec = pl.BlockSpec(memory_space=pl.ANY)
+    hbm_spec = pl.BlockSpec(memory_space=pltpu.HBM)
     in_specs = [
-        pl.BlockSpec(memory_space=pltpu.SMEM) if a is lengths else any_spec for a in operands
+        pl.BlockSpec(memory_space=pltpu.SMEM) if a is lengths else hbm_spec for a in operands
     ]
-    return pl.pallas_call(
+    shapes = ((rows, feats), (seqs, heads_here, key_dim), (seqs, heads_here, value_dim))
+    results = pl.pallas_call(
         functools.partial(layer_kernel, n_kv, n_tp, feats * n_kv),
-        out_shape=(
-            jax.ShapeDtypeStruct((rows, feats), BF16),
-            jax.ShapeDtypeStruct((seqs, heads_here, key_dim), BF16),
-            jax.ShapeDtypeStruct((seqs, heads_here, value_dim), BF16),
-        ),
+        out_shape=tuple(vmem(shape, BF16) for shape in shapes),
         in_specs=in_specs,
         out_specs=(pl.BlockSpec(memory_space=pltpu.VMEM),) * 3,
         scratch_shapes=scratch,
         compiler_params=pltpu.CompilerParams(
-            collective_id=0, has_side_effects=True, vmem_limit_bytes=60 * 1024 * 1024
+            collective_id=0, has_side_effects=True, vmem_limit_bytes=66900000
         ),
         name="layer",
     )(*operands)
+    local = (pl.BlockSpec(memory_space=pl.ANY),) * 3
+    return pl.pallas_call(
+        copy_out,
+        out_shape=tuple(jax.ShapeDtypeStruct(shape, BF16) for shape in shapes),
+        in_specs=local,
+        out_specs=local,
+        scratch_shapes=[dma((3,))],
+        name="results",
+    )(*results)
 
 
 def solution(mesh):

time: 54.7 us -> 45.3 us (0.83)
  local copies, waits for them, and re-layouts: 13 us -> 1.78 us
  Pallas kernels: 40.7 us -> 42.7 us
    unnamed x8 -> x6, local copies, waits for them, and re-layouts: 13 us -> 1.78 us
    pallas_call x0 -> x1, Pallas kernels: none -> 2.3 us  [on_device(): pl.pallas_call(copy_out, out_shape=tuple((jax.ShapeDtypeStruct(shape, BF1...]
where the time goes in v2:
time: 45.3 us; the launch traced here: 45.2 us
  Pallas kernels  42.7 us (94%)
  local copies, waits for them, and re-layouts  1.78 us (4%)
  between operations  0.66 us (1%)
    pallas_call x1, Pallas kernels, on_device(): pl.pallas_call(functools.partial(layer_kernel, n_kv, n_tp, feats * n_kv),...  40.4 us
    pallas_call x1, Pallas kernels, on_device(): pl.pallas_call(copy_out, out_shape=tuple((jax.ShapeDtypeStruct(shape, BF1...  2.3 us
    unnamed x6, local copies, waits for them, and re-layouts  1.78 us

profile of v2, /device:TPU:0, one launch (start us, length us, event | category | flops | bytes accessed | tf_op | source)
XLA Modules:
  0.0 45.2 jit_solution(14607715888663723003)
XLA Ops:
  0.6 40.4 %layer.1 = (bf16[32,512]{1,0:T(8,128)(2,1)S(1)}, bf16[4,2,128]{2,1,0:T(2,128)(2,1)S(1)}, bf16[4,2,256]{2,1,0:T(2,128)(2,1)S(1)}) custom-call(bf16[32,512]{1,0:T(8,128)(2,1)} %tokens_h.1, f32[1,512]{1,0:T(1,128)} %bitcast.10, bf16[512,256]{1,0:T(8,128)(2,1)} %wq_h.1, bf16[512,256]{1,0:T(8,128)(2,1)} %wk_h.1, bf16[512,512]{1,0:T(8,128)(2,1)} %wv_h.1, ...), custom_call_target="tpu_custom_call" | custom-call | tf_op jit(solution)/shard_map/layer/pallas_call | solution.py:492
  41.1 0.0 copy-start
  41.1 0.6 %copy-done = bf16[32,512]{1,0:T(8,128)(2,1)} copy-done((bf16[32,512]{1,0:T(8,128)(2,1)}, bf16[32,512]{1,0:T(8,128)(2,1)S(1)}, u32[]{:S(2)}) %copy-start) | copy-done | bytes 32792
  41.7 0.0 copy-start.2
  41.7 0.6 %copy-done.2 = bf16[4,2,128]{2,1,0:T(2,128)(2,1)} copy-done((bf16[4,2,128]{2,1,0:T(2,128)(2,1)}, bf16[4,2,128]{2,1,0:T(2,128)(2,1)S(1)}, u32[]{:S(2)}) %copy-start.2) | copy-done | bytes 2072
  42.3 0.0 copy-start.1
  42.3 0.6 %copy-done.1 = bf16[4,2,256]{2,1,0:T(2,128)(2,1)} copy-done((bf16[4,2,256]{2,1,0:T(2,128)(2,1)}, bf16[4,2,256]{2,1,0:T(2,128)(2,1)S(1)}, u32[]{:S(2)}) %copy-start.1) | copy-done | bytes 4120
  42.9 2.3 %results.1 = (bf16[32,512]{1,0:T(8,128)(2,1)}, bf16[4,2,128]{2,1,0:T(2,128)(2,1)}, bf16[4,2,256]{2,1,0:T(2,128)(2,1)}) custom-call(bf16[32,512]{1,0:T(8,128)(2,1)} %copy-done, bf16[4,2,128]{2,1,0:T(2,128)(2,1)} %copy-done.2, bf16[4,2,256]{2,1,0:T(2,128)(2,1)} %copy-done.1), custom_call_target="tpu_custom_call" | custom-call | tf_op jit(solution)/shard_map/results/pallas_call | solution.py:504
Async XLA Ops:
  41.1 0.6 %copy-start = (bf16[32,512]{1,0:T(8,128)(2,1)}, bf16[32,512]{1,0:T(8,128)(2,1)S(1)}, u32[]{:S(2)}) copy-start(bf16[32,512]{1,0:T(8,128)(2,1)S(1)} %get-tuple-element.6.refs_0_) | copy-start | bytes 98308
  41.7 0.6 %copy-start.2 = (bf16[4,2,128]{2,1,0:T(2,128)(2,1)}, bf16[4,2,128]{2,1,0:T(2,128)(2,1)S(1)}, u32[]{:S(2)}) copy-start(bf16[4,2,128]{2,1,0:T(2,128)(2,1)S(1)} %get-tuple-element.7.refs_1_) | copy-start | bytes 6148
  42.3 0.6 %copy-start.1 = (bf16[4,2,256]{2,1,0:T(2,128)(2,1)}, bf16[4,2,256]{2,1,0:T(2,128)(2,1)S(1)}, u32[]{:S(2)}) copy-start(bf16[4,2,256]{2,1,0:T(2,128)(2,1)S(1)} %get-tuple-element.8.refs_2_) | copy-start | bytes 12292
